TPU v7x, 32 devices: a whole 2x2x4 slice. The times are simulated.
32 devices in a mesh: fs: 8 (over z, x), tp: 4 (over y, core).
Axes of the slice: x: 2, y: 2, z: 4, core: 2. Of those that a mesh axis runs over, the one named last changes fastest.
Arguments:
- tokens: bfloat16 [1024, 2048], P('fs', 'tp'), may hold values from -6 to 6
- routes: int32 [1024, 2], P('fs'), may hold values from 0 to 3, all different within a row; in each aligned block of 128 rows (0 to 127, 128 to 255, ...) at most 96 rows name the same one
- route_weight: float32 [1024, 2], P('fs'), may hold values from 0.1 to 1
- norm_gain: float32 [2048], P('fs'), may hold values from 0.1 to 1.9
- expert_gate: float32 [4, 2048, 512], P(None, 'fs', 'tp'), may hold values from -0.125 to 0.125
- expert_up: float32 [4, 2048, 512], P(None, 'fs', 'tp'), may hold values from -0.125 to 0.125
- expert_down: float32 [4, 2048, 512], P(None, 'fs', 'tp'), may hold values from -0.25 to 0.25
- shared_gate: float32 [2048, 512], P('fs', 'tp'), may hold values from -0.125 to 0.125
- shared_up: float32 [2048, 512], P('fs', 'tp'), may hold values from -0.125 to 0.125
- shared_down: float32 [512, 2048], P('tp', 'fs'), may hold values from -0.25 to 0.25
Outputs:
- mixed: bfloat16 [1024, 2048], P('fs', 'tp')
- gate_sampler: bfloat16 [8, 2048, 256], P('fs', None, 'tp')
- up_sampler: bfloat16 [8, 2048, 256], P('fs', None, 'tp')
- down_sampler: bfloat16 [8, 2048, 256], P('fs', 'tp')
- shared_gate_out: bfloat16 [2048, 512], P(None, 'tp')
- shared_up_out: bfloat16 [2048, 512], P(None, 'tp')
- shared_down_out: bfloat16 [512, 2048], P('tp')
Inputs may be any that keep to these rules, and one draw needn't show every extreme that they name: `routes`: each row names 2 different experts. In each aligned block of 128 rows no expert is named by more than 96 rows, a bound that some block reaches.
All inputs are finite; a program needn't handle non-finite values.
Results may differ from a plain program's by a relative error of at most 0.009.
Values may be sent and summed in bfloat16 or wider, within the bound.
A program may use at most 64 MiB of HBM per device.

v0:
```python
import jax
import jax.numpy as jnp
from jax import lax
from jax.sharding import PartitionSpec as P

EPS = 1e-06


def to_owners(matrix, expert_count, unit_count):
    row_share = matrix.shape[1]
    return (
        matrix.reshape(expert_count, row_share, 2, unit_count)
        .transpose(0, 2, 1, 3)
        .reshape(2 * expert_count, row_share, unit_count)
    )


def on_device(
    tokens,
    routes,
    route_weight,
    norm_gain,
    expert_gate,
    expert_up,
    expert_down,
    shared_gate,
    shared_up,
    shared_down,
):
    fs_count = lax.axis_size("fs")
    tp_count = lax.axis_size("tp")
    expert_count, row_share, col_share = expert_gate.shape
    unit_count = col_share // 2
    model_width = row_share * fs_count
    quarter = model_width // tp_count
    tok_count, pick_count = routes.shape
    capacity = 2 * ((3 * tok_count * pick_count + 4 * expert_count - 1) // (4 * expert_count))
    slot_count = fs_count * capacity
    row_gain = norm_gain[None, :, None]
    gate_owned = to_owners((expert_gate * row_gain).astype(jnp.bfloat16), expert_count, unit_count)
    up_owned = to_owners((expert_up * row_gain).astype(jnp.bfloat16), expert_count, unit_count)
    gate_new, up_new = (
        lax.all_to_all(gate_owned, "fs", split_axis=0, concat_axis=1, tiled=True),
        lax.all_to_all(up_owned, "fs", split_axis=0, concat_axis=1, tiled=True),
    )
    down_owned = to_owners(expert_down.astype(jnp.bfloat16), expert_count, unit_count)
    down_new = lax.all_to_all(
        lax.all_to_all(down_owned, "fs", split_axis=0, concat_axis=1, tiled=True),
        "tp",
        split_axis=1,
        concat_axis=2,
        tiled=True,
    )
    shared_gate_new, shared_up_new, shared_down_new = (
        lax.all_gather(
            (shared_gate * norm_gain[:, None]).astype(jnp.bfloat16), "fs", axis=0, tiled=True
        ),
        lax.all_gather(
            (shared_up * norm_gain[:, None]).astype(jnp.bfloat16), "fs", axis=0, tiled=True
        ),
        lax.all_gather(shared_down.astype(jnp.bfloat16), "fs", axis=1, tiled=True),
    )
    gathered = lax.all_gather(tokens, "tp", axis=1, tiled=True)
    tokens_wide = gathered.astype(jnp.float32)
    normed = (
        tokens_wide * lax.rsqrt(jnp.mean(tokens_wide * tokens_wide, axis=1, keepdims=True) + EPS)
    ).astype(jnp.bfloat16)
    shared_act = jnp.dot(normed, shared_gate_new, preferred_element_type=jnp.float32)
    shared_lin = jnp.dot(normed, shared_up_new, preferred_element_type=jnp.float32)
    shared_hidden = (jax.nn.silu(shared_act) * shared_lin).astype(jnp.bfloat16)
    shared_term = jnp.dot(shared_hidden, shared_down_new, preferred_element_type=jnp.float32)
    shared_sum = lax.psum_scatter(
        shared_term.astype(jnp.bfloat16), "tp", scatter_dimension=1, tiled=True
    ).astype(jnp.float32)
    assigned = routes.reshape(-1)
    onehot = (assigned[:, None] == jnp.arange(expert_count, dtype=jnp.int32)[None, :]).astype(
        jnp.int32
    )
    earlier = jnp.cumsum(onehot, axis=0) - onehot
    position = jnp.sum(earlier * onehot, axis=1)
    slot_index = assigned * capacity + position
    token_index = jnp.arange(tok_count * pick_count, dtype=jnp.int32) // pick_count
    slot_token = (
        jnp.full((expert_count * capacity,), tok_count, jnp.int32).at[slot_index].set(token_index)
    )
    padded = jnp.concatenate([normed, jnp.zeros((1, model_width), jnp.bfloat16)], axis=0)
    own_part = lax.dynamic_slice_in_dim(padded, lax.axis_index("tp") * quarter, quarter, 1)
    outgoing = jnp.repeat(
        own_part[slot_token].reshape(expert_count, capacity, quarter), 2, axis=0
    ).reshape(slot_count, quarter)
    arrived = lax.all_to_all(outgoing, "fs", split_axis=0, concat_axis=0, tiled=True)
    portion = lax.all_gather(arrived, "tp", axis=1, tiled=True)
    gate_rows = gate_new[0]
    up_rows = up_new[0]
    gate_act = jnp.dot(portion, gate_rows, preferred_element_type=jnp.float32)
    up_act = jnp.dot(portion, up_rows, preferred_element_type=jnp.float32)
    hidden = (jax.nn.silu(gate_act) * up_act).astype(jnp.bfloat16)
    down_cols = down_new[0]
    half_sum = lax.dot_general(
        lax.all_gather(hidden, "tp", axis=1, tiled=True),
        down_cols,
        (((1,), (1,)), ((), ())),
        preferred_element_type=jnp.float32,
    )
    returned = lax.all_to_all(
        half_sum.astype(jnp.bfloat16), "fs", split_axis=0, concat_axis=0, tiled=True
    )
    pair_sum = jnp.sum(
        returned.astype(jnp.float32).reshape(expert_count, 2, capacity, quarter), axis=1
    ).reshape(expert_count * capacity, quarter)
    gathered_slots = pair_sum[slot_index].reshape(tok_count, pick_count, quarter)
    routed = jnp.sum(gathered_slots * route_weight[:, :, None], axis=1)
    mixed = (shared_sum + routed).astype(jnp.bfloat16)
    return (mixed, gate_new, up_new, down_new, shared_gate_new, shared_up_new, shared_down_new)


def solution(mesh):
    in_specs = (
        P("fs", "tp"),
        P("fs", None),
        P("fs", None),
        P("fs"),
        P(None, "fs", "tp"),
        P(None, "fs", "tp"),
        P(None, "fs", "tp"),
        P("fs", "tp"),
        P("fs", "tp"),
        P("tp", "fs"),
    )
    out_specs = (
        P("fs", "tp"),
        P("fs", None, "tp"),
        P("fs", None, "tp"),
        P("fs", "tp", None),
        P(None, "tp"),
        P(None, "tp"),
        P("tp", None),
    )
    return jax.shard_map(
        on_device, mesh=mesh, in_specs=in_specs, out_specs=out_specs, check_vma=False
    )
```

profile of v0, /device:TPU:9, one launch (start us, length us, event | category | flops | bytes accessed | tf_op | source)
XLA Modules:
  0.0 256.2 jit_solution(7877371888522557811)
XLA Ops:
  9.0 7.9 %all_gather.18 = bf16[128,2048]{1,0:T(8,128)(2,1)S(1)} all-gather(bf16[128,512]{1,0:T(8,128)(2,1)} %param.10), channel_id=1, replica_groups=mesh['fs'=8,'tp'=4] {'tp'}, dimensions={1}, use_global_device_ids=true | all-gather | bytes 655360 | tf_op jit(solution)/shard_map/all_gather | solution.py:63
  17.3 1.2 reduce-window.6
  19.2 1.4 scatter_custom_fusion
  20.7 2.1 gather_fusion
  22.8 24.1 %all_to_all.75 = bf16[8,96,512]{2,1,0:T(8,128)(2,1)} all-to-all(bf16[8,96,512]{2,1,0:T(8,128)(2,1)S(1)} %bitcast.62), channel_id=1, replica_groups=mesh['fs'=8,'tp'=4] {'fs'}, dimensions={0} | all-to-all | bytes 1572864 | tf_op jit(solution)/shard_map/all_to_all | solution.py:91
  48.4 5.3 %all-to-all-start.1 = ((bf16[8,256,64]{1,2,0:T(8,128)(2,1)}), bf16[8,256,64]{1,2,0:T(8,128)(2,1)S(1)}, u32[]{:S(2)}, u32[]{:S(2)}) async-start(bf16[8,256,64]{1,2,0:T(8,128)(2,1)} %copy.50), calls=%async_computation.2 | async-start | bytes 524288 | tf_op jit(solution)/shard_map/all_to_all | solution.py:43
  54.9 5.2 %all-to-all-done.1 = bf16[8,256,64]{1,2,0:T(8,128)(2,1)S(1)} async-done(((bf16[8,256,64]{1,2,0:T(8,128)(2,1)}), bf16[8,256,64]{1,2,0:T(8,128)(2,1)S(1)}, u32[]{:S(2)}, u32[]{:S(2)}) %all-to-all-start.1) | async-done | bytes 262176 | tf_op jit(solution)/shard_map/all_to_all | solution.py:43
  60.1 5.8 %all-to-all-start.3 = ((bf16[8,256,64]{1,2,0:T(8,128)(2,1)}), bf16[8,256,64]{1,2,0:T(8,128)(2,1)S(1)}, u32[]{:S(2)}, u32[]{:S(2)}) async-start(bf16[8,256,64]{1,2,0:T(8,128)(2,1)} %copy.56), calls=%async_computation.4 | async-start | bytes 524288 | tf_op jit(solution)/shard_map/all_to_all | solution.py:48
  66.9 4.8 %all-to-all-done.3 = bf16[8,256,64]{1,2,0:T(8,128)(2,1)S(1)} async-done(((bf16[8,256,64]{1,2,0:T(8,128)(2,1)}), bf16[8,256,64]{1,2,0:T(8,128)(2,1)S(1)}, u32[]{:S(2)}, u32[]{:S(2)}) %all-to-all-start.3) | async-done | bytes 262176 | tf_op jit(solution)/shard_map/all_to_all | solution.py:48
  71.7 6.3 %all-to-all-start.2 = ((bf16[8,256,64]{1,2,0:T(8,128)(2,1)}), bf16[8,256,64]{1,2,0:T(8,128)(2,1)S(1)}, u32[]{:S(2)}, u32[]{:S(2)}) async-start(bf16[8,256,64]{1,2,0:T(8,128)(2,1)} %copy.53), calls=%async_computation.3 | async-start | bytes 524288 | tf_op jit(solution)/shard_map/all_to_all | solution.py:44
  78.1 25.2 %all_gather.19 = bf16[2048,128]{1,0:T(8,128)(2,1)S(1)} all-gather(bf16[256,128]{1,0:T(8,128)(2,1)S(1)} %get-tuple-element.34), channel_id=1, replica_groups=mesh['fs'=8,'tp'=4] {'fs'}, dimensions={0}, use_global_device_ids=true | all-gather | bytes 589824 | tf_op jit(solution)/shard_map/all_gather | solution.py:55
  104.4 11.5 %reduce = bf16[2048,64]{1,0:T(8,128)(2,1)S(1)} reduce(bf16[2048,1,64]{2,1,0:T(2,128)(2,1)S(1)} %bitcast.60, bf16[]{:T(256)} %broadcast.90), dimensions={1}, to_apply=%bitcast.45.reduce_sub_computation | reduce | bytes 524290
  115.9 1.1 reshape.151
  117.0 10.1 %all-to-all-start.4 = ((bf16[4,2,16384]{2,1,0:T(2,128)(2,1)}), bf16[4,2,16384]{2,1,0:T(2,128)(2,1)S(1)}, u32[]{:S(2)}, u32[]{:S(2)}) async-start(bf16[4,2,16384]{2,1,0:T(2,128)(2,1)} %reshape.151), calls=%async_computation.5 | async-start | bytes 524288 | tf_op jit(solution)/shard_map/all_to_all | solution.py:47
  127.1 25.3 %all_gather.20 = bf16[2048,128]{1,0:T(8,128)(2,1)S(1)} all-gather(bf16[256,128]{1,0:T(8,128)(2,1)S(1)} %get-tuple-element.35), channel_id=1, replica_groups=mesh['fs'=8,'tp'=4] {'fs'}, dimensions={0}, use_global_device_ids=true | all-gather | bytes 589824 | tf_op jit(solution)/shard_map/all_gather | solution.py:58
  155.4 3.1 %fusion.20 = f32[768,64]{0,1:T(8,128)S(1)} fusion(bf16[768,2048]{1,0:T(8,128)(2,1)} %all-gather.2.cloned.1.call-done, bf16[2048,64]{0,1:T(8,128)(2,1)} %bitcast.71), kind=kOutput, calls=%fused_computation.54 | convolution fusion | flops 201326592 | bytes 3604480 | tf_op jit(solution)/shard_map/dot_general | solution.py:95
  159.6 13.3 %all_gather.23 = bf16[768,256]{0,1:T(8,128)(2,1)S(1)} all-gather(bf16[768,64]{0,1:T(8,128)(2,1)S(1)} %fusion), channel_id=1, replica_groups=mesh['fs'=8,'tp'=4] {'tp'}, dimensions={1}, use_global_device_ids=true | all-gather | bytes 491520 | tf_op jit(solution)/shard_map/all_gather | solution.py:100
  173.0 1.3 convolution_convert_fusion.1
  174.3 7.2 %all-to-all-start.5 = ((bf16[8,96,512]{2,1,0:T(8,128)(2,1)}), bf16[8,96,512]{2,1,0:T(8,128)(2,1)}, u32[]{:S(2)}, u32[]{:S(2)}) async-start(bf16[8,96,512]{2,1,0:T(8,128)(2,1)} %bitcast.12), calls=%async_computation.6 | async-start | bytes 1572864 | tf_op jit(solution)/shard_map/all_to_all | solution.py:105
  181.5 34.6 %all_gather.21 = bf16[128,2048]{1,0:T(8,128)(2,1)S(1)} all-gather(bf16[128,256]{1,0:T(8,128)(2,1)S(1)} %convert_element_type.61), channel_id=1, replica_groups=mesh['fs'=8,'tp'=4] {'fs'}, dimensions={1}, use_global_device_ids=true | all-gather | bytes 589824 | tf_op jit(solution)/shard_map/all_gather | solution.py:61
  216.4 1.3 convolution_convert_fusion
  220.6 1.3 convert_reduce_fusion
  224.0 21.4 %reduce-scatter.2.cloned.1.call-done = bf16[128,512]{1,0:T(8,128)(2,1)} async-done(((bf16[128,2048]{1,0:T(8,128)(2,1)}), bf16[128,512]{1,0:T(8,128)(2,1)}) %reduce-scatter.2.cloned.1.call-update) | async-done | bytes 131088 | tf_op jit(solution)/shard_map/reduce_scatter | solution.py:72
  245.4 1.6 add_convert_fusion
  (87 shorter events, 19.3 us)
Async XLA Ops:
  7.2 148.2 %all-gather.2.cloned.1.call-start = ((), (), s32[]{:S(2)}) async-start(), calls=%async_computation.8 | async-start | bytes 3932160 | tf_op jit(solution)/shard_map/all_gather | solution.py:92
  20.6 26.3 %copy-start.2 = (f32[4,256,128]{2,1,0:T(8,128)S(1)}, f32[4,256,128]{2,1,0:T(8,128)}, u32[]{:S(2)}) copy-start(f32[4,256,128]{2,1,0:T(8,128)} %param.14) | copy-start | bytes 1572868
  20.6 26.3 %copy-start.3 = (f32[4,256,128]{2,1,0:T(8,128)S(1)}, f32[4,256,128]{2,1,0:T(8,128)}, u32[]{:S(2)}) copy-start(f32[4,256,128]{2,1,0:T(8,128)} %param.15) | copy-start | bytes 1572868
  20.6 26.3 %copy-start.8 = (f32[256]{0:T(256)S(1)}, f32[256]{0:T(256)}, u32[]{:S(2)}) copy-start(f32[256]{0:T(256)} %param.13) | copy-start | bytes 3076
  46.9 6.8 %copy-start.1 = (f32[4,256,128]{2,1,0:T(8,128)S(1)}, f32[4,256,128]{2,1,0:T(8,128)}, u32[]{:S(2)}) copy-start(f32[4,256,128]{2,1,0:T(8,128)} %param.16) | copy-start | bytes 1572868
  48.4 11.7 %all-to-all-start.1 = ((bf16[8,256,64]{1,2,0:T(8,128)(2,1)}), bf16[8,256,64]{1,2,0:T(8,128)(2,1)S(1)}, u32[]{:S(2)}, u32[]{:S(2)}) async-start(bf16[8,256,64]{1,2,0:T(8,128)(2,1)} %copy.50), calls=%async_computation.2 | async-start | bytes 524288 | tf_op jit(solution)/shard_map/all_to_all | solution.py:43
  53.7 13.2 %copy-start.7 = (f32[128,256]{1,0:T(8,128)S(1)}, f32[128,256]{1,0:T(8,128)}, u32[]{:S(2)}) copy-start(f32[128,256]{1,0:T(8,128)} %param.19) | copy-start | bytes 393220
  53.7 24.3 %copy-start.5 = (f32[256,128]{1,0:T(8,128)S(1)}, f32[256,128]{1,0:T(8,128)}, u32[]{:S(2)}) copy-start(f32[256,128]{1,0:T(8,128)} %param.17) | copy-start | bytes 393220
  53.7 24.3 %copy-start.6 = (f32[256,128]{1,0:T(8,128)S(1)}, f32[256,128]{1,0:T(8,128)}, u32[]{:S(2)}) copy-start(f32[256,128]{1,0:T(8,128)} %param.18) | copy-start | bytes 393220
  60.1 11.6 %all-to-all-start.3 = ((bf16[8,256,64]{1,2,0:T(8,128)(2,1)}), bf16[8,256,64]{1,2,0:T(8,128)(2,1)S(1)}, u32[]{:S(2)}, u32[]{:S(2)}) async-start(bf16[8,256,64]{1,2,0:T(8,128)(2,1)} %copy.56), calls=%async_computation.4 | async-start | bytes 524288 | tf_op jit(solution)/shard_map/all_to_all | solution.py:48
  71.7 45.3 %all-to-all-start.2 = ((bf16[8,256,64]{1,2,0:T(8,128)(2,1)}), bf16[8,256,64]{1,2,0:T(8,128)(2,1)S(1)}, u32[]{:S(2)}, u32[]{:S(2)}) async-start(bf16[8,256,64]{1,2,0:T(8,128)(2,1)} %copy.53), calls=%async_computation.3 | async-start | bytes 524288 | tf_op jit(solution)/shard_map/all_to_all | solution.py:44
  117.0 36.9 %all-to-all-start.4 = ((bf16[4,2,16384]{2,1,0:T(2,128)(2,1)}), bf16[4,2,16384]{2,1,0:T(2,128)(2,1)S(1)}, u32[]{:S(2)}, u32[]{:S(2)}) async-start(bf16[4,2,16384]{2,1,0:T(2,128)(2,1)} %reshape.151), calls=%async_computation.5 | async-start | bytes 524288 | tf_op jit(solution)/shard_map/all_to_all | solution.py:47
  155.1 3.4 %copy-start.4 = (bf16[8,8,8,256]{3,2,0,1:T(8,128)(2,1)S(1)}, bf16[8,8,8,256]{3,2,0,1:T(8,128)(2,1)}, u32[]{:S(2)}) copy-start(bf16[8,8,8,256]{3,2,0,1:T(8,128)(2,1)} %copy.75) | copy-start | bytes 786436
  155.4 3.1 %copy-start = (bf16[768,2048]{1,0:T(8,128)(2,1)S(1)}, bf16[768,2048]{1,0:T(8,128)(2,1)}, u32[]{:S(2)}) copy-start(bf16[768,2048]{1,0:T(8,128)(2,1)} %all-gather.2.cloned.1.call-done) | copy-start | bytes 9437188
  174.2 43.5 %copy-start.9 = (f32[128,2]{0,1:T(2,128)S(1)}, f32[128,2]{0,1:T(2,128)}, u32[]{:S(2)}) copy-start(f32[128,2]{0,1:T(2,128)} %param.12) | copy-start | bytes 3076
  174.3 46.4 %all-to-all-start.5 = ((bf16[8,96,512]{2,1,0:T(8,128)(2,1)}), bf16[8,96,512]{2,1,0:T(8,128)(2,1)}, u32[]{:S(2)}, u32[]{:S(2)}) async-start(bf16[8,96,512]{2,1,0:T(8,128)(2,1)} %bitcast.12), calls=%async_computation.6 | async-start | bytes 1572864 | tf_op jit(solution)/shard_map/all_to_all | solution.py:105
  181.5 63.9 %reduce-scatter.2.cloned.1.call-start = ((), (), s32[]{:S(2)}) async-start(), calls=%async_computation.7 | async-start | bytes 655360 | tf_op jit(solution)/shard_map/reduce_scatter | solution.py:72
Sparse Core Ops, SparseCore 0:
  47.0 29.1 all-gather.1
  217.8 27.5 reduce-scatter.1
where the time goes:
time: 259 us; the launch traced here: 256 us
  blocking collectives  130 us (50%)
  starting transfers between devices  34.8 us (13%)
  waiting for transfers between devices  31.4 us (12%)
  local copies, waits for them, and re-layouts  19.9 us (8%)
  other arithmetic  18.2 us (7%)
  between operations  14.4 us (6%)
  matrix products  7.1 us (3%)
    all_gather x1, blocking collectives, on_device(): lax.all_gather(shared_down.astype(jnp.bfloat16), 'fs', axis=1, tiled=True)  34.6 us
    all_gather x1, blocking collectives, on_device(): lax.all_gather((shared_up * norm_gain[:, None]).astype(jnp.bfloat16), 'fs...  25.3 us
    all_gather x1, blocking collectives, on_device(): lax.all_gather((shared_gate * norm_gain[:, None]).astype(jnp.bfloat16), '...  25.2 us
    all_to_all x1, blocking collectives, on_device(): lax.all_to_all(outgoing, 'fs', split_axis=0, concat_axis=0, tiled=True)  24.1 us
    reduce_scatter x1, waiting for transfers between devices, on_device(): lax.psum_scatter(shared_term.astype(jnp.bfloat16), 'tp', scatter_dimensio...  21.4 us
    all_gather x1, blocking collectives, on_device(): lax.all_gather(hidden, 'tp', axis=1, tiled=True)  13.3 us
    unnamed x2, other arithmetic  11.6 us
    all_to_all x1, starting transfers between devices, on_device(): lax.all_to_all(lax.all_to_all(down_owned, 'fs', split_axis=0, concat_axis...  10.1 us
  transfers between devices with their start and end apart: 7, of which 3 were waited for; matrix products, arithmetic and copies ran while one was open for 10% of the time, Pallas kernels for 0%

commit v1 on v0

v1 whole, which is shorter than its diff:
```python
import functools

import jax
import jax.numpy as jnp
from jax import lax
from jax.experimental import pallas as pl
from jax.experimental.pallas import tpu as pltpu
from jax.sharding import PartitionSpec as P

EPS = 1e-06
BF = jnp.bfloat16
F32 = jnp.float32


def loop(low, high, body):
    def step(i, carry):
        body(i)
        return carry

    lax.fori_loop(low, high, step, 0)


def dot(a, b):
    return jnp.dot(a, b, preferred_element_type=F32)


def dot_nt(a, b):
    return lax.dot_general(a, b, (((1,), (1,)), ((), ())), preferred_element_type=F32)


def left_halves(a, b, half):
    lane = lax.broadcasted_iota(jnp.int32, a.shape, 1)
    return jnp.where(lane < half, a, pltpu.roll(b, half, 1))


def right_halves(a, b, half):
    lane = lax.broadcasted_iota(jnp.int32, a.shape, 1)
    return jnp.where(lane < half, pltpu.roll(a, half, 1), b)


def silu(v):
    return v / (1.0 + jnp.exp(-v))


def kernel(
    F,
    T,
    slots,
    tok,
    routes,
    weight,
    gain,
    eg,
    eu,
    ed,
    sg,
    su,
    sd,
    mixed,
    gu_out,
    dn_out,
    sg_out,
    su_out,
    sd_out,
    tk,
    nm,
    gu_send,
    gu,
    dn_send,
    dn,
    sh,
    disp,
    port,
    hid,
    ret_send,
    ret,
    part,
    shr,
    s_tok,
    r_tok,
    s_gu,
    r_gu,
    s_dn,
    r_dn,
    s_sha,
    s_shb,
    r_sh,
    s_da,
    s_db,
    s_out,
    s_in,
    r_port,
    s_hid,
    r_hid,
    s_ret,
    r_ret,
    s_shr,
    r_shr,
):
    G = F // 2
    K = F // T
    E = eg.shape[0]
    R, C = eg.shape[1], eg.shape[2]
    half = C // 2
    tok_count = tok.shape[0]
    quarter = tok.shape[1]
    width = quarter * T
    f = lax.axis_index("fs")
    t = lax.axis_index("tp")
    g, p = f // 2, f % 2
    pair = g * 2 + (1 - p)
    t_pair = (t // 2) * 2 + (1 - t % 2)

    def remote(src, dst, send, recv, fs, tp):
        return pltpu.make_async_remote_copy(
            src_ref=src,
            dst_ref=dst,
            send_sem=send,
            recv_sem=recv,
            device_id={"fs": fs, "tp": tp},
            device_id_type=pl.DeviceIdType.MESH,
        )

    def arrived(dst, send, recv):
        remote(dst, dst, send, recv, pair, t).wait_recv()

    def sent(src, send, recv):
        remote(src, src, send, recv, pair, t).wait_send()

    def send_tok(d):
        remote(tok, tk.at[t], s_tok.at[d], r_tok.at[t], f, (t + d) % T).start()

    loop(1, T, send_tok)
    tk[t] = tok[...]

    gains = gain[...]

    def fold(e):
        gate, up = eg[e] * gains, eu[e] * gains
        gu_send[2 * e] = left_halves(gate, up, half).astype(BF)
        gu_send[2 * e + 1] = right_halves(gate, up, half).astype(BF)

    loop(0, E, fold)
    gu[f] = gu_send[f]

    def send_gu(d):
        j = (f + d) % F
        remote(gu_send.at[j], gu.at[f], s_gu.at[d], r_gu.at[f], j, t).start()

    loop(1, F, send_gu)

    def fold_down(e):
        top, low = ed[e, : R // 2], ed[e, R // 2 :]
        dn_send[2 * e] = left_halves(top, low, half).astype(BF)
        dn_send[2 * e + 1] = right_halves(top, low, half).astype(BF)

    loop(0, E, fold_down)
    sh[f, 0] = (sg[...] * gains).astype(BF)
    sh[f, 1] = (su[...] * gains).astype(BF)
    sh[f, 2] = sd[...].T.astype(BF)

    experts = lax.broadcasted_iota(jnp.int32, (tok_count, E), 1)
    first, second = routes[:, 0:1], routes[:, 1:2]
    named = ((experts == first) | (experts == second)).astype(F32)
    rows = lax.broadcasted_iota(jnp.int32, (tok_count, tok_count), 0)
    cols = lax.broadcasted_iota(jnp.int32, (tok_count, tok_count), 1)
    before = (cols < rows).astype(F32).astype(BF)
    place = dot(before, named.astype(BF))
    slot_ids = lax.broadcasted_iota(jnp.int32, (tok_count, E * slots), 1)

    def pick_of(chosen):
        spot = jnp.sum(jnp.where(experts == chosen, place, 0.0), axis=1, keepdims=True)
        return slot_ids == chosen * slots + spot.astype(jnp.int32)

    pick0, pick1 = pick_of(first), pick_of(second)
    both = jnp.where(pick0 | pick1, 1.0, 0.0).astype(BF)

    def wait_tok(d):
        src = (t + d) % T
        arrived(tk.at[src], s_tok.at[d], r_tok.at[src])

    loop(1, T, wait_tok)
    squares = jnp.zeros((tok_count, 1), F32)
    for q in range(T):
        x = tk[q].astype(F32)
        squares = squares + jnp.sum(x * x, axis=1, keepdims=True)
    scale = lax.rsqrt(squares / width + EPS)
    for q in range(T):
        nm[q] = (tk[q].astype(F32) * scale).astype(BF)

    packed = lax.dot_general(
        both, nm[t], (((0,), (0,)), ((), ())), preferred_element_type=F32
    ).astype(BF)
    disp[...] = packed.reshape(E, slots, quarter)
    port[t, f] = disp[g]

    def send_disp(d):
        e = (g + d) % G
        remote(
            disp.at[e], port.at[t, f], s_da.at[d], r_port.at[t, f], 2 * e + p, t
        ).start()

    loop(1, G, send_disp)

    def send_shared(d):
        remote(
            sh.at[f], sh.at[f], s_sha.at[d], r_sh.at[f], ((g + d) % G) * 2 + p, t
        ).start()

    def pass_block(block):
        for d in range(1, T // 2):
            remote(
                port.at[t, block],
                port.at[t, block],
                s_out.at[d, block],
                r_port.at[t, block],
                f,
                (t + 2 * d) % T,
            ).start()
        remote(
            port.at[t, block],
            port.at[t, block],
            s_in.at[0, block],
            r_port.at[t, block],
            f,
            t_pair,
        ).start()

    def direct_block(d):
        block = ((g + d) % G) * 2 + p

        @pl.when(d > 0)
        def _():
            arrived(port.at[t, block], s_da.at[d], r_port.at[t, block])

        remote(
            port.at[t, block],
            port.at[t, block],
            s_db.at[d],
            r_port.at[t, block],
            pair,
            t,
        ).start()
        pass_block(block)

    def pair_block(d):
        block = ((g + d) % G) * 2 + 1 - p
        arrived(port.at[t, block], s_db.at[d], r_port.at[t, block])
        pass_block(block)

    def inner_block(d):
        for o in range(1, T // 2):
            src = (t + 2 * o) % T
            for q in (p, 1 - p):
                block = ((g + d) % G) * 2 + q
                arrived(port.at[src, block], s_out.at[o, block], r_port.at[src, block])
                remote(
                    port.at[src, block],
                    port.at[src, block],
                    s_in.at[o, block],
                    r_port.at[src, block],
                    f,
                    t_pair,
                ).start()

    def down_copy(d):
        j = (f + d) % F
        return remote(
            dn_send.at[j], dn.at[f % K, t], s_dn.at[d], r_dn.at[f % K, t], j, f // K
        )

    mine = f // K == t

    @pl.when(mine)
    def _():
        dn[f % K, t] = dn_send[f]

    def send_down(d):
        @pl.when(jnp.logical_not((d == 0) & mine))
        def _():
            down_copy(d).start()

    loop(0, F, send_down)
    loop(1, G, send_shared)
    remote(sh.at[f], sh.at[f], s_shb.at[0], r_sh.at[f], pair, t).start()
    loop(0, G, direct_block)
    loop(0, G, pair_block)

    def pass_shared(d):
        block = ((g + d) % G) * 2 + p
        arrived(sh.at[block], s_sha.at[d], r_sh.at[block])
        remote(sh.at[block], sh.at[block], s_shb.at[d], r_sh.at[block], pair, t).start()

    loop(1, G, pass_shared)
    loop(0, G, inner_block)

    def wait_shared(d):
        block = ((g + d) % G) * 2 + 1 - p
        arrived(sh.at[block], s_shb.at[d], r_sh.at[block])

    loop(0, G, wait_shared)

    gate_sh = sh[:, 0].reshape(F * R, C)
    up_sh = sh[:, 1].reshape(F * R, C)
    down_sh = sh[:, 2].reshape(F * R, C)
    sg_out[...] = gate_sh
    su_out[...] = up_sh
    sd_out[...] = down_sh.astype(F32).T.astype(BF)
    act = jnp.zeros((tok_count, C), F32)
    lin = jnp.zeros((tok_count, C), F32)
    for q in range(T):
        act = act + dot(nm[q], gate_sh[q * quarter : (q + 1) * quarter])
        lin = lin + dot(nm[q], up_sh[q * quarter : (q + 1) * quarter])
    hidden_sh = (silu(act) * lin).astype(BF)
    for q in range(T):
        part[q] = dot_nt(hidden_sh, down_sh[q * quarter : (q + 1) * quarter]).astype(BF)
    shr[t] = part[t]

    def send_part(d):
        q = (t + d) % T
        remote(part.at[q], shr.at[t], s_shr.at[d], r_shr.at[t], f, q).start()

    loop(1, T, send_part)

    def wait_gu(d):
        src = (f + d) % F
        arrived(gu.at[src], s_gu.at[d], r_gu.at[src])

    loop(1, F, wait_gu)
    gu_out[...] = gu[...].reshape(F * R, C)

    def hidden_of(block):
        total = jnp.zeros((slots, C), F32)
        for q in range(T):
            total = total + dot(port[q, block], gu_out[q * quarter : (q + 1) * quarter, :])
        return silu(total) * pltpu.roll(total, half, 1)

    def wait_inner(block):
        for o in range(T // 2):
            src = (t_pair + 2 * o) % T
            arrived(port.at[src, block], s_in.at[o, block], r_port.at[src, block])

    def expert_hidden(d):
        group = (g + d) % G
        wait_inner(2 * group)
        wait_inner(2 * group + 1)
        hid[t, group] = left_halves(
            hidden_of(2 * group), hidden_of(2 * group + 1), half
        ).astype(BF)
        for o in range(1, T):
            remote(
                hid.at[t, group],
                hid.at[t, group],
                s_hid.at[o, group],
                r_hid.at[t, group],
                f,
                (t + o) % T,
            ).start()

    loop(0, G, expert_hidden)

    def wait_down(k):
        for q in range(T):

            @pl.when(jnp.logical_not((t * K + k == f) & (t == q)))
            def _():
                arrived(dn.at[k, q], s_dn.at[0], r_dn.at[k, q])

    loop(0, K, wait_down)

    def place_down(k):
        for q in range(0, T, 2):
            a, b = dn[k, q].astype(F32), dn[k, q + 1].astype(F32)
            block = jnp.concatenate([left_halves(a, b, half), right_halves(a, b, half)], axis=0)
            dn_out[pl.ds(pl.multiple_of(k * R, R), R), q * half : (q + 2) * half] = block.astype(BF)

    loop(0, K, place_down)

    def ret_copy(d, q):
        block = ((g + d) % G) * 2 + q
        return block, remote(
            ret_send.at[block], ret.at[p, g], s_ret.at[block], r_ret.at[p, g], block, t
        )

    def expert_out(d):
        group = (g + d) % G
        for o in range(1, T):
            src = (t + o) % T
            arrived(hid.at[src, group], s_hid.at[o, group], r_hid.at[src, group])
        out_a = jnp.zeros((slots, quarter), F32)
        out_b = jnp.zeros((slots, quarter), F32)
        for q in range(0, T, 2):
            a, b = hid[q, group].astype(F32), hid[q + 1, group].astype(F32)
            down = dn_out[:, q * half : (q + 2) * half]
            out_a = out_a + dot_nt(left_halves(a, b, half).astype(BF), down)
            out_b = out_b + dot_nt(right_halves(a, b, half).astype(BF), down)
        ret_send[2 * group] = out_a.astype(BF)
        ret_send[2 * group + 1] = out_b.astype(BF)
        for q in range(2):
            block, copy = ret_copy(d, q)

            @pl.when(block != f)
            def _():
                copy.start()

    loop(0, G, expert_out)
    ret[p, g] = ret_send[f]

    def wait_part(d):
        src = (t + d) % T
        arrived(shr.at[src], s_shr.at[d], r_shr.at[src])

    loop(1, T, wait_part)
    total = shr[0].astype(F32)
    for q in range(1, T):
        total = total + shr[q].astype(F32)

    def wait_ret(d):
        src = (f + d) % F
        arrived(ret.at[src % 2, src // 2], s_ret.at[src], r_ret.at[src % 2, src // 2])

    loop(1, F, wait_ret)
    for k, pick in enumerate((pick0, pick1)):
        chosen = jnp.where(pick, 1.0, 0.0).astype(BF)
        halves = dot(chosen, ret[0].reshape(E * slots, quarter)) + dot(
            chosen, ret[1].reshape(E * slots, quarter)
        )
        total = total + weight[:, k : k + 1] * halves
    mixed[...] = total.astype(BF)

    def done_tp(d):
        sent(tok, s_tok.at[d], r_tok.at[0])
        sent(part.at[0], s_shr.at[d], r_shr.at[0])

        def inner(group):
            sent(hid.at[t, group], s_hid.at[d, group], r_hid.at[0, 0])

        loop(0, G, inner)

    loop(1, T, done_tp)

    def done_fs(d):
        sent(gu_send.at[0], s_gu.at[d], r_gu.at[0])
        sent(ret_send.at[0], s_ret.at[(f + d) % F], r_ret.at[0, 0])

    loop(1, F, done_fs)

    def done_down(d):
        @pl.when(jnp.logical_not((d == 0) & mine))
        def _():
            sent(dn_send.at[0], s_dn.at[d], r_dn.at[0, 0])

    loop(0, F, done_down)

    def done_groups(d):
        sent(sh.at[f], s_shb.at[d], r_sh.at[0])
        sent(disp.at[0], s_db.at[d], r_port.at[0, 0])

        @pl.when(d > 0)
        def _():
            sent(sh.at[f], s_sha.at[d], r_sh.at[0])
            sent(disp.at[0], s_da.at[d], r_port.at[0, 0])

    loop(0, G, done_groups)

    def done_blocks(block):
        for o in range(T // 2):
            sent(disp.at[0], s_in.at[o, block], r_port.at[0, 0])
            if o > 0:
                sent(disp.at[0], s_out.at[o, block], r_port.at[0, 0])

    loop(0, F, done_blocks)


def on_device(
    tokens,
    routes,
    route_weight,
    norm_gain,
    expert_gate,
    expert_up,
    expert_down,
    shared_gate,
    shared_up,
    shared_down,
):
    F = lax.axis_size("fs")
    T = lax.axis_size("tp")
    E, R, C = expert_gate.shape
    tok_count, quarter = tokens.shape
    pick_count = routes.shape[1]
    capacity = 2 * ((3 * tok_count * pick_count + 4 * E - 1) // (4 * E))
    slots = (capacity + 15) // 16 * 16
    G, K = F // 2, F // T
    vmem = pl.BlockSpec(memory_space=pltpu.VMEM)
    dma = pltpu.SemaphoreType.DMA
    shapes = [
        (tok_count, quarter),
        (F * R, C),
        (K * R, T * C // 2),
        (F * R, C),
        (F * R, C),
        (C, F * R),
    ]
    scratch = [
        (T, tok_count, quarter),
        (T, tok_count, quarter),
        (F, R, C),
        (F, R, C),
        (F, R // 2, C),
        (K, T, R // 2, C),
        (F, 3, R, C),
        (E, slots, quarter),
        (T, F, slots, quarter),
        (T, G, slots, C),
        (F, slots, quarter),
        (2, E, slots, quarter),
        (T, tok_count, quarter),
        (T, tok_count, quarter),
    ]
    sems = [
        (T,), (T,), (F,), (F,), (F,), (K, T), (G,), (G,), (F,), (G,), (G,),
        (T // 2, F), (T // 2, F), (T, F), (T, G), (T, G), (F,), (2, E), (T,), (T,),
    ]
    mixed, gu, down, sg, su, sd = pl.pallas_call(
        functools.partial(kernel, F, T, slots),
        out_shape=[jax.ShapeDtypeStruct(s, BF) for s in shapes],
        in_specs=[vmem] * 10,
        out_specs=[vmem] * 6,
        scratch_shapes=[pltpu.VMEM(s, BF) for s in scratch] + [dma(s) for s in sems],
        compiler_params=pltpu.CompilerParams(
            has_side_effects=True, vmem_limit_bytes=60 * 1024 * 1024
        ),
    )(
        tokens,
        routes,
        route_weight,
        norm_gain[:, None],
        expert_gate,
        expert_up,
        expert_down,
        shared_gate,
        shared_up,
        shared_down,
    )
    return (mixed, gu[None, :, : C // 2], gu[None, :, C // 2 :], down[None], sg, su, sd)


def solution(mesh):
    in_specs = (
        P("fs", "tp"),
        P("fs", None),
        P("fs", None),
        P("fs"),
        P(None, "fs", "tp"),
        P(None, "fs", "tp"),
        P(None, "fs", "tp"),
        P("fs", "tp"),
        P("fs", "tp"),
        P("tp", "fs"),
    )
    out_specs = (
        P("fs", "tp"),
        P("fs", None, "tp"),
        P("fs", None, "tp"),
        P("fs", "tp", None),
        P(None, "tp"),
        P(None, "tp"),
        P("tp", None),
    )
    return jax.shard_map(
        on_device, mesh=mesh, in_specs=in_specs, out_specs=out_specs, check_vma=False
    )
```

time: 259 us -> 110 us (0.42)
  blocking collectives: 130 us -> 0 us
  Pallas kernels: 0 us -> 96.4 us
  starting transfers between devices: 34.8 us -> 0 us
  waiting for transfers between devices: 31.4 us -> 0 us
  other arithmetic: 18.2 us -> 0 us
  between operations: 14.4 us -> 0.66 us
  local copies, waits for them, and re-layouts: 19.9 us -> 10.8 us
  matrix products: 7.1 us -> 0 us
    all_gather x5 -> x0, blocking collectives: 106 us -> none  [the longest x1 34.6 us: on_device(): lax.all_gather(shared_down.astype(jnp.bfloat16), 'fs', axis=1, tiled=True)]
    pallas_call x0 -> x1, Pallas kernels: none -> 96.4 us  [on_device(): pl.pallas_call(functools.partial(kernel, F, T, slots), out_shape=[jax.Sha...]
    all_to_all x5 -> x0, starting transfers between devices: 34.8 us -> none  [the longest x1 10.1 us: on_device(): lax.all_to_all(lax.all_to_all(down_owned, 'fs', split_axis=0, concat_axis...]
    all_to_all x1 -> x0, blocking collectives: 24.1 us -> none  [on_device(): lax.all_to_all(outgoing, 'fs', split_axis=0, concat_axis=0, tiled=True)]
    reduce_scatter x1 -> x0, waiting for transfers between devices: 21.4 us -> none  [on_device(): lax.psum_scatter(shared_term.astype(jnp.bfloat16), 'tp', scatter_dimensio...]
    unnamed x2 -> x0, other arithmetic: 11.6 us -> none
    all_to_all x5 -> x0, waiting for transfers between devices: 9.95 us -> none  [the longest x1 5.18 us: on_device(): lax.all_to_all(gate_owned, 'fs', split_axis=0, concat_axis=1, tiled=True)]
    dot_general x5 -> x0, matrix products: 7.1 us -> none  [the longest x1 3.12 us: on_device(): gate_act = jnp.dot(portion, gate_rows, preferred_element_type=jnp.float32)]
  transfers between devices with their start and end apart: 7 -> 0, of which waited for: 3 -> 0; matrix products, arithmetic and copies ran while one was open for 10% -> 0% of each run, Pallas kernels for 0% -> 0%
where the time goes in v1:
time: 110 us; the launch traced here: 108 us
  Pallas kernels  96.4 us (88%)
  local copies, waits for them, and re-layouts  10.8 us (10%)
    pallas_call x1, Pallas kernels, on_device(): pl.pallas_call(functools.partial(kernel, F, T, slots), out_shape=[jax.Sha...  96.4 us
    unnamed x25, local copies, waits for them, and re-layouts  8.58 us

profile of v1, /device:TPU:9, one launch (start us, length us, event | category | flops | bytes accessed | tf_op | source)
XLA Modules:
  0.0 107.9 jit_solution(15114593060749458660)
XLA Ops:
  0.6 0.0 copy-start.5
  0.6 0.7 copy-done.5
  1.3 0.0 copy-start.6
  1.3 0.7 copy.21.routes
  2.1 0.0 copy-done.6
  2.1 0.0 copy-start.7
  2.1 0.7 copy.22.weight
  2.8 0.0 copy-done.7
  2.8 0.8 copy.23.gain
  3.6 96.4 %shard_map.153 = (bf16[128,512]{1,0:T(8,128)(2,1)}, bf16[2048,128]{1,0:T(8,128)(2,1)}, bf16[512,256]{1,0:T(8,128)(2,1)}, bf16[2048,128]{1,0:T(8,128)(2,1)}, bf16...) custom-call(bf16[128,512]{1,0:T(8,128)(2,1)} %tok.1, s32[128,2]{1,0:T(8,128)} %copy.21.routes, f32[128,2]{1,0:T(8,128)} %copy.22.weight, ...), custom_call_target="tpu_custom_call" | custom-call | tf_op jit(solution)/shard_map/pallas_call | solution.py:525
  100.0 1.4 %slice_bitcast_fusion = (bf16[1,2048,64]{2,1,0:T(8,128)(2,1)S(1)}, bf16[1,2048,64]{2,1,0:T(8,128)(2,1)S(1)}) fusion(bf16[2048,128]{1,0:T(8,128)(2,1)} %get-tuple-element.14), kind=kLoop, calls=%fused_computation | loop fusion | bytes 1048576 | tf_op jit(solution)/shard_map/broadcast_in_dim | solution.py:546
  101.4 0.9 copy.25
  102.3 0.0 copy-start.4
  102.3 0.9 copy.24
  103.2 0.0 copy-done.4
  103.2 0.7 copy.31
  103.9 0.0 copy-done.3
  103.9 0.7 copy.32
  104.6 0.0 copy-done.2
  104.6 0.8 copy.33
  105.4 0.4 copy-done.1
  105.8 0.8 copy.34
  106.6 0.4 copy-done
  107.1 0.8 copy.35
  (4 shorter events, 0.0 us)
Async XLA Ops:
  0.6 0.7 copy-start.5
  1.3 0.7 copy-start.6
  2.1 0.7 copy-start.7
  102.3 0.9 copy-start.4
  102.3 1.6 %copy-start.3 = (bf16[512,256]{1,0:T(8,128)(2,1)S(1)}, bf16[512,256]{1,0:T(8,128)(2,1)}, u32[]{:S(2)}) copy-start(bf16[512,256]{1,0:T(8,128)(2,1)} %get-tuple-element.15) | copy-start | bytes 786436
  103.2 1.4 %copy-start.2 = (bf16[2048,128]{1,0:T(8,128)(2,1)S(1)}, bf16[2048,128]{1,0:T(8,128)(2,1)}, u32[]{:S(2)}) copy-start(bf16[2048,128]{1,0:T(8,128)(2,1)} %get-tuple-element.46) | copy-start | bytes 1572868
  104.6 1.2 %copy-start.1 = (bf16[2048,128]{1,0:T(8,128)(2,1)S(1)}, bf16[2048,128]{1,0:T(8,128)(2,1)}, u32[]{:S(2)}) copy-start(bf16[2048,128]{1,0:T(8,128)(2,1)} %get-tuple-element.47) | copy-start | bytes 1572868
  105.8 1.2 %copy-start = (bf16[128,2048]{1,0:T(8,128)(2,1)S(1)}, bf16[128,2048]{1,0:T(8,128)(2,1)}, u32[]{:S(2)}) copy-start(bf16[128,2048]{1,0:T(8,128)(2,1)} %get-tuple-element.48) | copy-start | bytes 1572868

commit v2 on v1

--- a/solution.py
+++ b/solution.py
@@ -57,7 +57,8 @@
     su,
     sd,
     mixed,
-    gu_out,
+    gate_out,
+    up_out,
     dn_out,
     sg_out,
     su_out,
@@ -72,6 +73,9 @@
     disp,
     port,
     hid,
+    away,
+    keep,
+    near,
     ret_send,
     ret,
     part,
@@ -82,7 +86,8 @@
     r_gu,
     s_dn,
     r_dn,
-    s_sha,
+    s_left,
+    s_right,
     s_shb,
     r_sh,
     s_da,
@@ -92,6 +97,8 @@
     r_port,
     s_hid,
     r_hid,
+    s_near,
+    r_near,
     s_ret,
     r_ret,
     s_shr,
@@ -133,7 +140,7 @@
     loop(1, T, send_tok)
     tk[t] = tok[...]
 
-    gains = gain[...]
+    gains = jnp.broadcast_to(gain[...], (8, R)).T[:, 0:1]
 
     def fold(e):
         gate, up = eg[e] * gains, eu[e] * gains
@@ -160,7 +167,12 @@
     sh[f, 2] = sd[...].T.astype(BF)
 
     experts = lax.broadcasted_iota(jnp.int32, (tok_count, E), 1)
-    first, second = routes[:, 0:1], routes[:, 1:2]
+    line = lax.broadcasted_iota(jnp.int32, (8, tok_count), 0)
+    named_by = routes[...].astype(F32)
+    turned = jnp.where(line == 0, named_by[0:1], named_by[1:2])
+    turned = jnp.where(line == 2, weight[0:1, :], turned)
+    turned = jnp.where(line == 3, weight[1:2, :], turned).T
+    first, second = turned[:, 0:1].astype(jnp.int32), turned[:, 1:2].astype(jnp.int32)
     named = ((experts == first) | (experts == second)).astype(F32)
     rows = lax.broadcasted_iota(jnp.int32, (tok_count, tok_count), 0)
     cols = lax.broadcasted_iota(jnp.int32, (tok_count, tok_count), 1)
@@ -202,10 +214,36 @@
 
     loop(1, G, send_disp)
 
-    def send_shared(d):
-        remote(
-            sh.at[f], sh.at[f], s_sha.at[d], r_sh.at[f], ((g + d) % G) * 2 + p, t
-        ).start()
+    def shared_copy(block, sems, to):
+        return remote(sh.at[block], sh.at[block], sems, r_sh.at[block], to, t)
+
+    def share_left(block):
+        @pl.when(g > 0)
+        def _():
+            shared_copy(block, s_left.at[block // 2], f - 2).start()
+
+    def share_right(block):
+        @pl.when(g < G - 1)
+        def _():
+            shared_copy(block, s_right.at[block // 2], f + 2).start()
+
+    def share_pair(block):
+        shared_copy(block, s_shb.at[block // 2], pair).start()
+
+    def relay(k):
+        @pl.when(g - k >= 0)
+        def _():
+            block = f - 2 * k
+            arrived(sh.at[block], s_right.at[0], r_sh.at[block])
+            share_right(block)
+            share_pair(block)
+
+        @pl.when(g + k < G)
+        def _():
+            block = f + 2 * k
+            arrived(sh.at[block], s_left.at[0], r_sh.at[block])
+            share_left(block)
+            share_pair(block)
 
     def pass_block(block):
         for d in range(1, T // 2):
@@ -280,59 +318,27 @@
         def _():
             down_copy(d).start()
 
+    share_left(f)
+    share_right(f)
     loop(0, F, send_down)
-    loop(1, G, send_shared)
-    remote(sh.at[f], sh.at[f], s_shb.at[0], r_sh.at[f], pair, t).start()
     loop(0, G, direct_block)
     loop(0, G, pair_block)
-
-    def pass_shared(d):
-        block = ((g + d) % G) * 2 + p
-        arrived(sh.at[block], s_sha.at[d], r_sh.at[block])
-        remote(sh.at[block], sh.at[block], s_shb.at[d], r_sh.at[block], pair, t).start()
-
-    loop(1, G, pass_shared)
+    share_pair(f)
+    relay(1)
     loop(0, G, inner_block)
-
-    def wait_shared(d):
-        block = ((g + d) % G) * 2 + 1 - p
-        arrived(sh.at[block], s_shb.at[d], r_sh.at[block])
-
-    loop(0, G, wait_shared)
-
-    gate_sh = sh[:, 0].reshape(F * R, C)
-    up_sh = sh[:, 1].reshape(F * R, C)
-    down_sh = sh[:, 2].reshape(F * R, C)
-    sg_out[...] = gate_sh
-    su_out[...] = up_sh
-    sd_out[...] = down_sh.astype(F32).T.astype(BF)
-    act = jnp.zeros((tok_count, C), F32)
-    lin = jnp.zeros((tok_count, C), F32)
-    for q in range(T):
-        act = act + dot(nm[q], gate_sh[q * quarter : (q + 1) * quarter])
-        lin = lin + dot(nm[q], up_sh[q * quarter : (q + 1) * quarter])
-    hidden_sh = (silu(act) * lin).astype(BF)
-    for q in range(T):
-        part[q] = dot_nt(hidden_sh, down_sh[q * quarter : (q + 1) * quarter]).astype(BF)
-    shr[t] = part[t]
-
-    def send_part(d):
-        q = (t + d) % T
-        remote(part.at[q], shr.at[t], s_shr.at[d], r_shr.at[t], f, q).start()
-
-    loop(1, T, send_part)
-
     def wait_gu(d):
         src = (f + d) % F
         arrived(gu.at[src], s_gu.at[d], r_gu.at[src])
 
     loop(1, F, wait_gu)
-    gu_out[...] = gu[...].reshape(F * R, C)
+
+    def rows_of(q):
+        return gu[q * K : (q + 1) * K].reshape(quarter, C)
 
     def hidden_of(block):
         total = jnp.zeros((slots, C), F32)
         for q in range(T):
-            total = total + dot(port[q, block], gu_out[q * quarter : (q + 1) * quarter, :])
+            total = total + dot(port[q, block], rows_of(q))
         return silu(total) * pltpu.roll(total, half, 1)
 
     def wait_inner(block):
@@ -359,6 +365,32 @@
 
     loop(0, G, expert_hidden)
 
+    def wait_shared(d):
+        block = ((g + d) % G) * 2 + 1 - p
+        arrived(sh.at[block], s_shb.at[d], r_sh.at[block])
+
+    loop(2, G, relay)
+    loop(0, G, wait_shared)
+
+    gate_sh = sh[:, 0].reshape(F * R, C)
+    up_sh = sh[:, 1].reshape(F * R, C)
+    down_sh = sh[:, 2].reshape(F * R, C)
+    act = jnp.zeros((tok_count, C), F32)
+    lin = jnp.zeros((tok_count, C), F32)
+    for q in range(T):
+        act = act + dot(nm[q], gate_sh[q * quarter : (q + 1) * quarter])
+        lin = lin + dot(nm[q], up_sh[q * quarter : (q + 1) * quarter])
+    hidden_sh = (silu(act) * lin).astype(BF)
+    for q in range(T):
+        part[q] = dot_nt(hidden_sh, down_sh[q * quarter : (q + 1) * quarter]).astype(BF)
+    shr[t] = part[t]
+
+    def send_part(d):
+        q = (t + d) % T
+        remote(part.at[q], shr.at[t], s_shr.at[d], r_shr.at[t], f, q).start()
+
+    loop(1, T, send_part)
+
     def wait_down(k):
         for q in range(T):
 
@@ -376,10 +408,9 @@
 
     loop(0, K, place_down)
 
-    def ret_copy(d, q):
-        block = ((g + d) % G) * 2 + q
-        return block, remote(
-            ret_send.at[block], ret.at[p, g], s_ret.at[block], r_ret.at[p, g], block, t
+    def near_copy(group):
+        return remote(
+            away.at[group], near.at[group], s_near.at[group], r_near.at[group], pair, t
         )
 
     def expert_out(d):
@@ -394,17 +425,35 @@
             down = dn_out[:, q * half : (q + 2) * half]
             out_a = out_a + dot_nt(left_halves(a, b, half).astype(BF), down)
             out_b = out_b + dot_nt(right_halves(a, b, half).astype(BF), down)
-        ret_send[2 * group] = out_a.astype(BF)
-        ret_send[2 * group + 1] = out_b.astype(BF)
-        for q in range(2):
-            block, copy = ret_copy(d, q)
-
-            @pl.when(block != f)
-            def _():
-                copy.start()
+        even, odd = out_a.astype(BF), out_b.astype(BF)
+        keep[group] = jnp.where(p == 0, even, odd)
+        away[group] = jnp.where(p == 0, odd, even)
+        near_copy(group).start()
 
     loop(0, G, expert_out)
-    ret[p, g] = ret_send[f]
+
+    def add_halves(d):
+        group = (g + d) % G
+        arrived(near.at[group], s_near.at[group], r_near.at[group])
+        ret_send[group] = (keep[group].astype(F32) + near[group].astype(F32)).astype(BF)
+        remote(
+            ret_send.at[group], ret.at[g], s_ret.at[group], r_ret.at[g], 2 * group + p, t
+        ).start()
+
+    loop(1, G, add_halves)
+    arrived(near.at[g], s_near.at[g], r_near.at[g])
+    ret[g] = (keep[g].astype(F32) + near[g].astype(F32)).astype(BF)
+
+    for q in range(T):
+        span = slice(q * quarter, (q + 1) * quarter)
+        turned_gu = rows_of(q).astype(F32).T.astype(BF)
+        gate_out[:, span] = turned_gu[:half]
+        up_out[:, span] = turned_gu[half:]
+        sd_out[:, span] = (
+            sh[q * K : (q + 1) * K, 2].reshape(quarter, C).astype(F32).T.astype(BF)
+        )
+    sg_out[...] = sh[:, 0].reshape(F * R, C)
+    su_out[...] = sh[:, 1].reshape(F * R, C)
 
     def wait_part(d):
         src = (t + d) % T
@@ -416,16 +465,14 @@
         total = total + shr[q].astype(F32)
 
     def wait_ret(d):
-        src = (f + d) % F
-        arrived(ret.at[src % 2, src // 2], s_ret.at[src], r_ret.at[src % 2, src // 2])
-
-    loop(1, F, wait_ret)
+        src = (g + d) % G
+        arrived(ret.at[src], s_ret.at[src], r_ret.at[src])
+
+    loop(1, G, wait_ret)
+    outs = ret[...].reshape(E * slots, quarter)
     for k, pick in enumerate((pick0, pick1)):
         chosen = jnp.where(pick, 1.0, 0.0).astype(BF)
-        halves = dot(chosen, ret[0].reshape(E * slots, quarter)) + dot(
-            chosen, ret[1].reshape(E * slots, quarter)
-        )
-        total = total + weight[:, k : k + 1] * halves
+        total = total + turned[:, 2 + k : 3 + k] * dot(chosen, outs)
     mixed[...] = total.astype(BF)
 
     def done_tp(d):
@@ -441,7 +488,6 @@
 
     def done_fs(d):
         sent(gu_send.at[0], s_gu.at[d], r_gu.at[0])
-        sent(ret_send.at[0], s_ret.at[(f + d) % F], r_ret.at[0, 0])
 
     loop(1, F, done_fs)
 
@@ -455,11 +501,20 @@
     def done_groups(d):
         sent(sh.at[f], s_shb.at[d], r_sh.at[0])
         sent(disp.at[0], s_db.at[d], r_port.at[0, 0])
+        sent(away.at[0], s_near.at[d], r_near.at[0])
 
         @pl.when(d > 0)
         def _():
-            sent(sh.at[f], s_sha.at[d], r_sh.at[0])
             sent(disp.at[0], s_da.at[d], r_port.at[0, 0])
+            sent(ret_send.at[0], s_ret.at[(g + d) % G], r_ret.at[0])
+
+        @pl.when((d >= g) & (g > 0))
+        def _():
+            sent(sh.at[f], s_left.at[d], r_sh.at[0])
+
+        @pl.when((d <= g) & (g < G - 1))
+        def _():
+            sent(sh.at[f], s_right.at[d], r_sh.at[0])
 
     loop(0, G, done_groups)
 
@@ -470,6 +525,11 @@
                 sent(disp.at[0], s_out.at[o, block], r_port.at[0, 0])
 
     loop(0, F, done_blocks)
+
+
+def hand_on(count, *refs):
+    for i in range(count):
+        refs[count + i][...] = refs[i][...]
 
 
 def on_device(
@@ -496,7 +556,8 @@
     dma = pltpu.SemaphoreType.DMA
     shapes = [
         (tok_count, quarter),
-        (F * R, C),
+        (C // 2, F * R),
+        (C // 2, F * R),
         (K * R, T * C // 2),
         (F * R, C),
         (F * R, C),
@@ -513,29 +574,32 @@
         (E, slots, quarter),
         (T, F, slots, quarter),
         (T, G, slots, C),
-        (F, slots, quarter),
-        (2, E, slots, quarter),
+        (G, slots, quarter),
+        (G, slots, quarter),
+        (G, slots, quarter),
+        (G, slots, quarter),
+        (E, slots, quarter),
         (T, tok_count, quarter),
         (T, tok_count, quarter),
     ]
     sems = [
-        (T,), (T,), (F,), (F,), (F,), (K, T), (G,), (G,), (F,), (G,), (G,),
-        (T // 2, F), (T // 2, F), (T, F), (T, G), (T, G), (F,), (2, E), (T,), (T,),
+        (T,), (T,), (F,), (F,), (F,), (K, T), (G,), (G,), (G,), (F,), (G,), (G,),
+        (T // 2, F), (T // 2, F), (T, F), (T, G), (T, G), (G,), (G,), (G,), (E,), (T,), (T,),
     ]
-    mixed, gu, down, sg, su, sd = pl.pallas_call(
+    results = pl.pallas_call(
         functools.partial(kernel, F, T, slots),
         out_shape=[jax.ShapeDtypeStruct(s, BF) for s in shapes],
         in_specs=[vmem] * 10,
-        out_specs=[vmem] * 6,
+        out_specs=[vmem] * 7,
         scratch_shapes=[pltpu.VMEM(s, BF) for s in scratch] + [dma(s) for s in sems],
         compiler_params=pltpu.CompilerParams(
             has_side_effects=True, vmem_limit_bytes=60 * 1024 * 1024
         ),
     )(
         tokens,
-        routes,
-        route_weight,
-        norm_gain[:, None],
+        routes.T,
+        route_weight.T,
+        norm_gain[None, :],
         expert_gate,
         expert_up,
         expert_down,
@@ -543,7 +607,13 @@
         shared_up,
         shared_down,
     )
-    return (mixed, gu[None, :, : C // 2], gu[None, :, C // 2 :], down[None], sg, su, sd)
+    mixed, gate, up, down, sg, su, sd = pl.pallas_call(
+        functools.partial(hand_on, 7),
+        out_shape=[jax.ShapeDtypeStruct(s, BF) for s in shapes],
+        in_specs=[vmem] * 7,
+        out_specs=[vmem] * 7,
+    )(*results)
+    return (mixed, gate.T[None], up.T[None], down[None], sg, su, sd)
 
 
 def solution(mesh):

time: 110 us -> 85.8 us (0.78)
  the two profiles are of different devices: /device:TPU:9 before, /device:TPU:28 now
where the time goes in v2:
time: 85.8 us; the launch traced here: 85.6 us
  Pallas kernels  84.9 us (99%)
    pallas_call x1, Pallas kernels, on_device(): pl.pallas_call(functools.partial(kernel, F, T, slots), out_shape=[jax.Sha...  81.8 us
    pallas_call x1, Pallas kernels, on_device(): pl.pallas_call(functools.partial(hand_on, 7), out_shape=[jax.ShapeDtypeSt...  3.1 us

profile of v2, /device:TPU:28, one launch (start us, length us, event | category | flops | bytes accessed | tf_op | source)
XLA Modules:
  0.0 85.6 jit_solution(18042711588480035909)
XLA Ops:
  0.6 81.8 %shard_map.153 = (bf16[128,512]{1,0:T(8,128)(2,1)}, bf16[64,2048]{1,0:T(8,128)(2,1)}, bf16[64,2048]{1,0:T(8,128)(2,1)}, bf16[512,256]{1,0:T(8,128)(2,1)}, bf16[2...) custom-call(bf16[128,512]{1,0:T(8,128)(2,1)} %tok.1, s32[2,128]{1,0:T(2,128)} %bitcast.10, ...), custom_call_target="tpu_custom_call" | custom-call | tf_op jit(solution)/shard_map/pallas_call | solution.py:589
  82.5 3.1 %shard_map.154 = (bf16[128,512]{1,0:T(8,128)(2,1)}, bf16[64,2048]{1,0:T(8,128)(2,1)}, bf16[64,2048]{1,0:T(8,128)(2,1)}, bf16[512,256]{1,0:T(8,128)(2,1)}, bf16[2...) custom-call(bf16[128,512]{1,0:T(8,128)(2,1)} %get-tuple-element.21.refs_0_, ...), custom_call_target="tpu_custom_call" | custom-call | tf_op jit(solution)/shard_map/pallas_call | solution.py:610

commit v3 on v2

--- a/solution.py
+++ b/solution.py
@@ -134,37 +134,13 @@
     def sent(src, send, recv):
         remote(src, src, send, recv, pair, t).wait_send()
 
-    def send_tok(d):
-        remote(tok, tk.at[t], s_tok.at[d], r_tok.at[t], f, (t + d) % T).start()
-
-    loop(1, T, send_tok)
+    def tok_copy(src, sem, to):
+        return remote(tk.at[src], tk.at[src], sem, r_tok.at[src], f, to)
+
+    for o in range(1, T // 2):
+        remote(tok, tk.at[t], s_tok.at[o], r_tok.at[t], f, (t + 2 * o) % T).start()
+    remote(tok, tk.at[t], s_tok.at[T // 2], r_tok.at[t], f, t_pair).start()
     tk[t] = tok[...]
-
-    gains = jnp.broadcast_to(gain[...], (8, R)).T[:, 0:1]
-
-    def fold(e):
-        gate, up = eg[e] * gains, eu[e] * gains
-        gu_send[2 * e] = left_halves(gate, up, half).astype(BF)
-        gu_send[2 * e + 1] = right_halves(gate, up, half).astype(BF)
-
-    loop(0, E, fold)
-    gu[f] = gu_send[f]
-
-    def send_gu(d):
-        j = (f + d) % F
-        remote(gu_send.at[j], gu.at[f], s_gu.at[d], r_gu.at[f], j, t).start()
-
-    loop(1, F, send_gu)
-
-    def fold_down(e):
-        top, low = ed[e, : R // 2], ed[e, R // 2 :]
-        dn_send[2 * e] = left_halves(top, low, half).astype(BF)
-        dn_send[2 * e + 1] = right_halves(top, low, half).astype(BF)
-
-    loop(0, E, fold_down)
-    sh[f, 0] = (sg[...] * gains).astype(BF)
-    sh[f, 1] = (su[...] * gains).astype(BF)
-    sh[f, 2] = sd[...].T.astype(BF)
 
     experts = lax.broadcasted_iota(jnp.int32, (tok_count, E), 1)
     line = lax.broadcasted_iota(jnp.int32, (8, tok_count), 0)
@@ -187,21 +163,8 @@
     pick0, pick1 = pick_of(first), pick_of(second)
     both = jnp.where(pick0 | pick1, 1.0, 0.0).astype(BF)
 
-    def wait_tok(d):
-        src = (t + d) % T
-        arrived(tk.at[src], s_tok.at[d], r_tok.at[src])
-
-    loop(1, T, wait_tok)
-    squares = jnp.zeros((tok_count, 1), F32)
-    for q in range(T):
-        x = tk[q].astype(F32)
-        squares = squares + jnp.sum(x * x, axis=1, keepdims=True)
-    scale = lax.rsqrt(squares / width + EPS)
-    for q in range(T):
-        nm[q] = (tk[q].astype(F32) * scale).astype(BF)
-
     packed = lax.dot_general(
-        both, nm[t], (((0,), (0,)), ((), ())), preferred_element_type=F32
+        both, tok[...], (((0,), (0,)), ((), ())), preferred_element_type=F32
     ).astype(BF)
     disp[...] = packed.reshape(E, slots, quarter)
     port[t, f] = disp[g]
@@ -265,7 +228,7 @@
         ).start()
 
     def direct_block(d):
-        block = ((g + d) % G) * 2 + p
+        block = ((g + G - d) % G) * 2 + p
 
         @pl.when(d > 0)
         def _():
@@ -282,7 +245,7 @@
         pass_block(block)
 
     def pair_block(d):
-        block = ((g + d) % G) * 2 + 1 - p
+        block = ((g + G - d) % G) * 2 + 1 - p
         arrived(port.at[t, block], s_db.at[d], r_port.at[t, block])
         pass_block(block)
 
@@ -290,7 +253,7 @@
         for o in range(1, T // 2):
             src = (t + 2 * o) % T
             for q in (p, 1 - p):
-                block = ((g + d) % G) * 2 + q
+                block = ((g + G - d) % G) * 2 + q
                 arrived(port.at[src, block], s_out.at[o, block], r_port.at[src, block])
                 remote(
                     port.at[src, block],
@@ -301,6 +264,34 @@
                     t_pair,
                 ).start()
 
+    loop(0, 1, direct_block)
+
+    gains = jnp.broadcast_to(gain[...], (8, R)).T[:, 0:1]
+
+    def fold(e):
+        gate, up = eg[e] * gains, eu[e] * gains
+        gu_send[2 * e] = left_halves(gate, up, half).astype(BF)
+        gu_send[2 * e + 1] = right_halves(gate, up, half).astype(BF)
+
+    loop(0, E, fold)
+    gu[f] = gu_send[f]
+
+    def send_gu(d):
+        j = (f + d) % F
+        remote(gu_send.at[j], gu.at[f], s_gu.at[d], r_gu.at[f], j, t).start()
+
+    loop(1, F, send_gu)
+
+    def fold_down(e):
+        top, low = ed[e, : R // 2], ed[e, R // 2 :]
+        dn_send[2 * e] = left_halves(top, low, half).astype(BF)
+        dn_send[2 * e + 1] = right_halves(top, low, half).astype(BF)
+
+    loop(0, E, fold_down)
+    sh[f, 0] = (sg[...] * gains).astype(BF)
+    sh[f, 1] = (su[...] * gains).astype(BF)
+    sh[f, 2] = sd[...].T.astype(BF)
+
     def down_copy(d):
         j = (f + d) % F
         return remote(
@@ -318,14 +309,19 @@
         def _():
             down_copy(d).start()
 
+    loop(0, F, send_down)
     share_left(f)
     share_right(f)
-    loop(0, F, send_down)
-    loop(0, G, direct_block)
+    loop(1, G, direct_block)
     loop(0, G, pair_block)
     share_pair(f)
-    relay(1)
     loop(0, G, inner_block)
+
+    for o in range(1, T // 2):
+        src = (t + 2 * o) % T
+        arrived(tk.at[src], s_tok.at[o], r_tok.at[src])
+        tok_copy(src, s_tok.at[T // 2 + o], t_pair).start()
+
     def wait_gu(d):
         src = (f + d) % F
         arrived(gu.at[src], s_gu.at[d], r_gu.at[src])
@@ -337,8 +333,12 @@
 
     def hidden_of(block):
         total = jnp.zeros((slots, C), F32)
+        squares = jnp.zeros((slots, 1), F32)
         for q in range(T):
             total = total + dot(port[q, block], rows_of(q))
+            x = port[q, block].astype(F32)
+            squares = squares + jnp.sum(x * x, axis=1, keepdims=True)
+        total = total * lax.rsqrt(squares / width + EPS)
         return silu(total) * pltpu.roll(total, half, 1)
 
     def wait_inner(block):
@@ -347,7 +347,7 @@
             arrived(port.at[src, block], s_in.at[o, block], r_port.at[src, block])
 
     def expert_hidden(d):
-        group = (g + d) % G
+        group = (g + G - d) % G
         wait_inner(2 * group)
         wait_inner(2 * group + 1)
         hid[t, group] = left_halves(
@@ -365,31 +365,7 @@
 
     loop(0, G, expert_hidden)
 
-    def wait_shared(d):
-        block = ((g + d) % G) * 2 + 1 - p
-        arrived(sh.at[block], s_shb.at[d], r_sh.at[block])
-
-    loop(2, G, relay)
-    loop(0, G, wait_shared)
-
-    gate_sh = sh[:, 0].reshape(F * R, C)
-    up_sh = sh[:, 1].reshape(F * R, C)
-    down_sh = sh[:, 2].reshape(F * R, C)
-    act = jnp.zeros((tok_count, C), F32)
-    lin = jnp.zeros((tok_count, C), F32)
-    for q in range(T):
-        act = act + dot(nm[q], gate_sh[q * quarter : (q + 1) * quarter])
-        lin = lin + dot(nm[q], up_sh[q * quarter : (q + 1) * quarter])
-    hidden_sh = (silu(act) * lin).astype(BF)
-    for q in range(T):
-        part[q] = dot_nt(hidden_sh, down_sh[q * quarter : (q + 1) * quarter]).astype(BF)
-    shr[t] = part[t]
-
-    def send_part(d):
-        q = (t + d) % T
-        remote(part.at[q], shr.at[t], s_shr.at[d], r_shr.at[t], f, q).start()
-
-    loop(1, T, send_part)
+    loop(1, min(2, G), relay)
 
     def wait_down(k):
         for q in range(T):
@@ -414,7 +390,7 @@
         )
 
     def expert_out(d):
-        group = (g + d) % G
+        group = (g + G - d) % G
         for o in range(1, T):
             src = (t + o) % T
             arrived(hid.at[src, group], s_hid.at[o, group], r_hid.at[src, group])
@@ -431,6 +407,7 @@
         near_copy(group).start()
 
     loop(0, G, expert_out)
+    loop(2, min(3, G), relay)
 
     def add_halves(d):
         group = (g + d) % G
@@ -443,6 +420,43 @@
     loop(1, G, add_halves)
     arrived(near.at[g], s_near.at[g], r_near.at[g])
     ret[g] = (keep[g].astype(F32) + near[g].astype(F32)).astype(BF)
+
+    def wait_shared(d):
+        block = ((g + G - d) % G) * 2 + 1 - p
+        arrived(sh.at[block], s_shb.at[d], r_sh.at[block])
+
+    loop(3, G, relay)
+    loop(0, G, wait_shared)
+
+    for o in range(T // 2):
+        src = (t_pair + 2 * o) % T
+        arrived(tk.at[src], s_tok.at[o], r_tok.at[src])
+    squares = jnp.zeros((tok_count, 1), F32)
+    for q in range(T):
+        x = tk[q].astype(F32)
+        squares = squares + jnp.sum(x * x, axis=1, keepdims=True)
+    scale = lax.rsqrt(squares / width + EPS)
+    for q in range(T):
+        nm[q] = (tk[q].astype(F32) * scale).astype(BF)
+
+    gate_sh = sh[:, 0].reshape(F * R, C)
+    up_sh = sh[:, 1].reshape(F * R, C)
+    down_sh = sh[:, 2].reshape(F * R, C)
+    act = jnp.zeros((tok_count, C), F32)
+    lin = jnp.zeros((tok_count, C), F32)
+    for q in range(T):
+        act = act + dot(nm[q], gate_sh[q * quarter : (q + 1) * quarter])
+        lin = lin + dot(nm[q], up_sh[q * quarter : (q + 1) * quarter])
+    hidden_sh = (silu(act) * lin).astype(BF)
+    for q in range(T):
+        part[q] = dot_nt(hidden_sh, down_sh[q * quarter : (q + 1) * quarter]).astype(BF)
+    shr[t] = part[t]
+
+    def send_part(d):
+        q = (t + d) % T
+        remote(part.at[q], shr.at[t], s_shr.at[d], r_shr.at[t], f, q).start()
+
+    loop(1, T, send_part)
 
     for q in range(T):
         span = slice(q * quarter, (q + 1) * quarter)

time: 85.8 us -> 80.1 us (0.934)
  the two profiles are of different devices: /device:TPU:28 before, /device:TPU:9 now
where the time goes in v3:
time: 80.1 us; the launch traced here: 79.9 us
  Pallas kernels  79.3 us (99%)
    pallas_call x1, Pallas kernels, on_device(): pl.pallas_call(functools.partial(kernel, F, T, slots), out_shape=[jax.Sha...  76.2 us
    pallas_call x1, Pallas kernels, on_device(): pl.pallas_call(functools.partial(hand_on, 7), out_shape=[jax.ShapeDtypeSt...  3.1 us

profile of v3, /device:TPU:9, one launch (start us, length us, event | category | flops | bytes accessed | tf_op | source)
XLA Modules:
  0.0 79.9 jit_solution(15918554749897285184)
XLA Ops:
  0.6 76.2 %shard_map.153 = (bf16[128,512]{1,0:T(8,128)(2,1)}, bf16[64,2048]{1,0:T(8,128)(2,1)}, bf16[64,2048]{1,0:T(8,128)(2,1)}, bf16[512,256]{1,0:T(8,128)(2,1)}, bf16[2...) custom-call(bf16[128,512]{1,0:T(8,128)(2,1)} %tok.1, s32[2,128]{1,0:T(2,128)} %bitcast.10, ...), custom_call_target="tpu_custom_call" | custom-call | tf_op jit(solution)/shard_map/pallas_call | solution.py:603
  76.8 3.1 %shard_map.154 = (bf16[128,512]{1,0:T(8,128)(2,1)}, bf16[64,2048]{1,0:T(8,128)(2,1)}, bf16[64,2048]{1,0:T(8,128)(2,1)}, bf16[512,256]{1,0:T(8,128)(2,1)}, bf16[2...) custom-call(bf16[128,512]{1,0:T(8,128)(2,1)} %get-tuple-element.21.refs_0_, ...), custom_call_target="tpu_custom_call" | custom-call | tf_op jit(solution)/shard_map/pallas_call | solution.py:624
